TPU v7x, 32 devices: a whole 2x2x4 slice. The times are simulated.
32 devices in a mesh: sp: 8 (over z, y), tp: 4 (over x, core).
Axes of the slice: x: 2, y: 2, z: 4, core: 2. Of those that a mesh axis runs over, the one named last changes fastest.
Arguments:
- resid: bfloat16 [6144, 2048], P(('sp', 'tp')), may hold values from -6 to 6
- query: bfloat16 [6144, 1024], P('sp', 'tp'), may hold values from -6 to 6
- keys: bfloat16 [6144, 1024], P('sp', 'tp'), may hold values from -6 to 6
- values: bfloat16 [6144, 1024], P('sp', 'tp'), may hold values from -6 to 6
- out_gate: bfloat16 [6144, 1024], P(('sp', 'tp')), may hold values from -6 to 6
- forget_pre: float32 [4, 6144], P('tp', 'sp'), may hold values from 0 to 16
- input_pre: float32 [4, 6144], P('tp', 'sp'), may hold values from -4 to 130
- head_gain: float32 [1024], replicated, may hold values from 0.1 to 1.9
- out_proj: bfloat16 [1024, 2048], replicated, may hold values from -0.1875 to 0.1875
- ffn_gain: float32 [2048], replicated, may hold values from 0.1 to 1.9
- routes: int32 [6144, 2], P(('sp', 'tp')), may hold values from 0 to 7, all different within a row; in each aligned block of 96 rows (0 to 95, 96 to 191, ...) at most 48 rows name the same one
- route_scores: float32 [6144, 2], P(('sp', 'tp')), may hold values from 0.1 to 1
- w_gate: bfloat16 [8, 2048, 512], P('sp'), may hold values from -0.125 to 0.125
- w_up: bfloat16 [8, 2048, 512], P('sp'), may hold values from -0.125 to 0.125
- w_down: bfloat16 [8, 512, 2048], P('sp'), may hold values from -0.25 to 0.25
Outputs:
- layer_out: bfloat16 [6144, 2048], P(('sp', 'tp'))
Inputs may be any that keep to these rules, and one draw needn't show every extreme that they name: `routes`: each row names 2 different experts; in each aligned block of 96 rows no expert is named by more than 48 rows, a bound that some block reaches.
All inputs are finite; a program needn't handle non-finite values.
Results may differ from a plain program's by a relative error of at most 0.0095.
Values may be sent and summed in bfloat16 or wider, within the bound.
A program may use at most 128 MiB of HBM per device.

v0:
```python
import jax
import jax.numpy as jnp
from jax import lax
from jax.sharding import PartitionSpec as P

BLOCK = 64


EPS = 1e-06
FLOOR_LOG = -1e30
HIGHEST = lax.Precision.HIGHEST


def prefix(part, axis, combine, identity):
    place = lax.axis_index(axis)
    gathered = jax.tree.map(lambda a: lax.all_gather(a, axis), part)
    state = jax.tree.map(lambda a, e: jnp.zeros_like(a) + jnp.asarray(e, a.dtype), part, identity)

    def one(step, state):
        return combine(
            state, jax.tree.map(lambda a: lax.dynamic_index_in_dim(a, step, 0, False), gathered)
        )

    return lax.fori_loop(0, place, one, state)


def block_pass(query, keys, values, log_forget, log_input, state):
    seq_len, head_width = query.shape
    blocks = seq_len // BLOCK
    key_scale = head_width ** (-0.5)
    causal = jnp.tril(jnp.ones((BLOCK, BLOCK), dtype=bool))

    def block_step(state_in, inputs):
        state_mat, state_vec, max_log = state_in
        q_block, k_block, v_block, forget_blk, input_blk = inputs
        cum_log = jnp.cumsum(forget_blk)
        block_total = cum_log[-1]
        log_mat = jnp.where(
            causal, cum_log[:, None] - cum_log[None, :] + input_blk[None, :], -jnp.inf
        )
        inter_log = cum_log + max_log
        row_max = jnp.maximum(inter_log, jnp.max(log_mat, axis=1))
        weight_mat = jnp.exp(log_mat - row_max[:, None])
        carry_weight = jnp.exp(inter_log - row_max)
        scores = jnp.dot(q_block, k_block.T, preferred_element_type=jnp.float32) * key_scale
        weights_blk = (scores * weight_mat).astype(jnp.bfloat16)
        q_float = q_block.astype(jnp.float32)
        numerator = carry_weight[:, None] * jnp.dot(
            q_float, state_mat, precision=HIGHEST
        ) + jnp.dot(weights_blk, v_block, preferred_element_type=jnp.float32)
        denominator = carry_weight * jnp.dot(q_float, state_vec, precision=HIGHEST) + jnp.sum(
            weights_blk.astype(jnp.float32), axis=1
        )
        log_keep = block_total - cum_log + input_blk
        new_max = jnp.maximum(block_total + max_log, jnp.max(log_keep))
        keep_weight = jnp.exp(log_keep - new_max)
        decay_now = jnp.exp(block_total + max_log - new_max)
        k_float = k_block.astype(jnp.float32) * key_scale
        state_mat = decay_now * state_mat + jnp.dot(
            (k_float * keep_weight[:, None]).T, v_block.astype(jnp.float32), precision=HIGHEST
        )
        state_vec = decay_now * state_vec + jnp.dot(keep_weight, k_float, precision=HIGHEST)
        return ((state_mat, state_vec, new_max), (numerator, denominator, row_max))

    def to_blocks(array_in):
        return array_in.reshape((blocks, BLOCK) + array_in.shape[1:])

    ignored, outputs = lax.scan(
        block_step,
        state,
        (
            to_blocks(query),
            to_blocks(keys),
            to_blocks(values),
            to_blocks(log_forget),
            to_blocks(log_input),
        ),
    )
    numerator, denominator, row_max = outputs
    return (
        numerator.reshape(seq_len, head_width),
        denominator.reshape(seq_len),
        row_max.reshape(seq_len),
    )


def end_state(keys, values, log_forget, log_input):
    head_width = keys.shape[1]
    cum_log = jnp.cumsum(log_forget)
    block_total = cum_log[-1]
    log_keep = block_total - cum_log + log_input
    max_log = jnp.max(log_keep)
    keep_weight = jnp.exp(log_keep - max_log)
    k_float = keys.astype(jnp.float32) * head_width ** (-0.5)
    state_mat = jnp.dot(
        (k_float * keep_weight[:, None]).T, values.astype(jnp.float32), precision=HIGHEST
    )
    state_vec = jnp.dot(keep_weight, k_float, precision=HIGHEST)
    return (state_mat, state_vec, max_log, block_total)


def join_states(earlier, latter):
    old_mat, old_vec, old_max, old_total = earlier
    new_mat, new_vec, new_max, new_total = latter
    joined_max = jnp.maximum(new_total + old_max, new_max)
    keep_old = jnp.exp(new_total + old_max - joined_max)
    keep_new = jnp.exp(new_max - joined_max)
    joined_mat = keep_old[:, None, None] * old_mat + keep_new[:, None, None] * new_mat
    joined_vec = keep_old[:, None] * old_vec + keep_new[:, None] * new_vec
    return (joined_mat, joined_vec, joined_max, old_total + new_total)


def slot_select(expert_ids, expert_count, capacity):
    flat_ids = expert_ids.reshape(-1)
    one_hot = (flat_ids[:, None] == jnp.arange(expert_count, dtype=jnp.int32)[None, :]).astype(
        jnp.int32
    )
    slot_rank = jnp.sum((jnp.cumsum(one_hot, axis=0) - 1) * one_hot, axis=1)
    target = flat_ids * capacity + slot_rank
    return (
        jnp.arange(expert_count * capacity, dtype=jnp.int32)[:, None] == target[None, :]
    ).astype(jnp.bfloat16)


def run_experts(arrived, w_gate, w_up, w_down, sources):
    local_count = w_gate.shape[0]
    grouped = arrived.reshape(sources, local_count, arrived.shape[1], arrived.shape[2])
    gate_pre = jnp.einsum("pesd,edf->pesf", grouped, w_gate, preferred_element_type=jnp.float32)
    up_pre = jnp.einsum("pesd,edf->pesf", grouped, w_up, preferred_element_type=jnp.float32)
    active = (jax.nn.silu(gate_pre) * up_pre).astype(jnp.bfloat16)
    result = jnp.einsum(
        "pesf,efd->pesd", active, w_down, preferred_element_type=jnp.float32
    ).astype(jnp.bfloat16)
    return result.reshape(arrived.shape)


def shards(
    resid,
    query,
    keys,
    values,
    out_gate,
    forget_pre,
    input_pre,
    head_gain,
    out_proj,
    ffn_gain,
    routes,
    route_scores,
    w_gate,
    w_up,
    w_down,
):
    local_heads = forget_pre.shape[0]
    seq_len = query.shape[0]
    head_width = query.shape[1] // local_heads
    log_forget = jax.nn.log_sigmoid(forget_pre)
    q_heads = query.reshape(seq_len, local_heads, head_width)
    k_heads = keys.reshape(seq_len, local_heads, head_width)
    v_heads = values.reshape(seq_len, local_heads, head_width)
    state_mat, state_vec, max_log, totals = jax.vmap(end_state, in_axes=(1, 1, 0, 0))(
        k_heads, v_heads, log_forget, input_pre
    )
    identity = (
        jnp.zeros((local_heads, head_width, head_width), jnp.float32),
        jnp.zeros((local_heads, head_width), jnp.float32),
        jnp.full((local_heads,), FLOOR_LOG, jnp.float32),
        jnp.zeros((local_heads,), jnp.float32),
    )
    carried = prefix((state_mat, state_vec, max_log, totals), "sp", join_states, identity)
    pass_heads = jax.vmap(block_pass, in_axes=(1, 1, 1, 0, 0, 0), out_axes=(1, 1, 1))
    numerator, denominator, row_max = pass_heads(
        q_heads, k_heads, v_heads, log_forget, input_pre, (identity[0], identity[1], identity[2])
    )
    cum_all = jnp.cumsum(log_forget, axis=1).T + carried[2][None, :]
    joined_max = jnp.maximum(row_max, cum_all)
    keep_own = jnp.exp(row_max - joined_max)
    keep_far = jnp.exp(cum_all - joined_max)
    q_float = q_heads.astype(jnp.float32)
    numerator = keep_own[:, :, None] * numerator + keep_far[:, :, None] * jnp.einsum(
        "lhd,hde->lhe", q_float, carried[0], precision=HIGHEST
    )
    denominator = keep_own * denominator + keep_far * jnp.einsum(
        "lhd,hd->lh", q_float, carried[1], precision=HIGHEST
    )
    row_max = joined_max
    hidden = numerator / jnp.maximum(jnp.abs(denominator), jnp.exp(-row_max))[:, :, None]
    cell_rows = hidden.reshape(seq_len, local_heads * head_width).astype(jnp.bfloat16)
    token_rows = lax.all_to_all(cell_rows, "tp", split_axis=0, concat_axis=1, tiled=True)
    cell_float = token_rows.astype(jnp.float32)
    headed = (
        cell_float
        * lax.rsqrt(jnp.mean(cell_float * cell_float, axis=1, keepdims=True) + EPS)
        * head_gain[None, :]
    )
    gated_out = (headed * jax.nn.sigmoid(out_gate.astype(jnp.float32))).astype(jnp.bfloat16)
    after_mix = resid.astype(jnp.float32) + jnp.dot(
        gated_out, out_proj, preferred_element_type=jnp.float32
    )
    normed_rows = (
        after_mix
        * lax.rsqrt(jnp.mean(after_mix * after_mix, axis=1, keepdims=True) + EPS)
        * ffn_gain[None, :]
    ).astype(jnp.bfloat16)
    row_count = normed_rows.shape[0]
    half_rows = row_count // 2
    route_count = routes.shape[1]
    sources = lax.axis_size("sp")
    expert_count = w_gate.shape[0] * sources
    capacity = max(2, 2 * half_rows * route_count // expert_count)
    selects = [
        slot_select(
            routes[half_idx * half_rows : (half_idx + 1) * half_rows], expert_count, capacity
        )
        for half_idx in range(2)
    ]

    def pack_rows(half_idx):
        selection = (
            selects[half_idx].reshape(expert_count * capacity, half_rows, route_count).sum(axis=2)
        )
        packed = jnp.dot(
            selection,
            normed_rows[half_idx * half_rows : (half_idx + 1) * half_rows],
            preferred_element_type=jnp.float32,
        )
        return packed.astype(jnp.bfloat16).reshape(expert_count, capacity, normed_rows.shape[1])

    send_rows = jnp.concatenate([pack_rows(0), pack_rows(1)], axis=1)
    finished = run_experts(
        lax.all_to_all(send_rows, "sp", split_axis=0, concat_axis=0, tiled=True),
        w_gate,
        w_up,
        w_down,
        sources,
    )
    returned = lax.all_to_all(finished, "sp", split_axis=0, concat_axis=0, tiled=True)
    answers = [returned[:, :capacity], returned[:, capacity:]]
    route_weight = route_scores / jnp.sum(route_scores, axis=1, keepdims=True)
    pieces = []
    for half_idx in range(2):
        gathered = lax.dot_general(
            selects[half_idx],
            answers[half_idx].reshape(expert_count * capacity, -1),
            (((0,), (0,)), ((), ())),
            preferred_element_type=jnp.float32,
        )
        weights_half = route_weight[half_idx * half_rows : (half_idx + 1) * half_rows]
        pieces.append(
            jnp.sum(gathered.reshape(half_rows, route_count, -1) * weights_half[:, :, None], axis=1)
        )
    return (after_mix + jnp.concatenate(pieces, axis=0)).astype(jnp.bfloat16)


def solution(mesh):
    placed = (
        P(("sp", "tp"), None),
        P("sp", "tp"),
        P("sp", "tp"),
        P("sp", "tp"),
        P(("sp", "tp"), None),
        P("tp", "sp"),
        P("tp", "sp"),
        P(),
        P(),
        P(),
        P(("sp", "tp"), None),
        P(("sp", "tp"), None),
        P("sp", None, None),
        P("sp", None, None),
        P("sp", None, None),
    )
    return jax.shard_map(
        shards, mesh=mesh, in_specs=placed, out_specs=P(("sp", "tp"), None), check_vma=False
    )
```

profile of v0, /device:TPU:0, one launch (start us, length us, event | category | flops | bytes accessed | tf_op | source)
XLA Modules:
  0.0 429.5 jit_solution(1679653552651287913)
XLA Ops:
  8.8 2.0 fusion.111
  11.4 2.8 fusion.79
  18.5 136.7 %while.38 = (s32[]{:T(128)}, f32[1,256,256]{2,1,0:T(8,128)S(1)}, f32[1,256]{1,0:T(1,128)S(1)}, f32[1]{0:T(128)}, f32[12,1,64,256]{3,2,1,0:T(8,128)}, /*index=5*/...) while((s32[]{:T(128)}, f32[1,256,256]{2,1,0:T(8,128)S(1)}, ...), condition=%wide.region_5.6_spmd.clone, body=%wide.region_0.5_spmd.clone.sunk | while | flops 105678720 | bytes 1283846 | solution.py:68
  24.5 1.6 fusion.158
  28.3 1.6 convolution_add_fusion.4
  35.9 1.6 fusion.158
  47.3 1.6 fusion.158
  51.1 1.6 convolution_add_fusion.4
  62.5 1.6 convolution_add_fusion.4
  73.8 1.6 convolution_add_fusion.4
  85.2 1.6 convolution_add_fusion.4
  92.9 1.6 fusion.158
  96.6 1.6 convolution_add_fusion.4
  108.0 1.6 convolution_add_fusion.4
  119.4 1.6 convolution_add_fusion.4
  130.8 1.6 convolution_add_fusion.4
  138.4 1.6 fusion.158
  142.2 1.6 convolution_add_fusion.4
  153.6 1.6 convolution_add_fusion.4
  155.2 23.8 %all-reduce.4 = (f32[8]{0:T(128)}, f32[8]{0:T(128)}) all-reduce(f32[8]{0:T(128)S(1)} %bitcast_dynamic-update-slice_fusion, f32[8]{0:T(128)S(1)} %dynamic-update-slice.1), channel_id=1, replica_groups=mesh['sp'=8,'tp'=4] {'sp'}, use_global_device_ids=true, to_apply=%add.2 | all-reduce | flops 16 | bytes 128
  186.8 16.3 %all-gather.2 = f32[8,1,256]{2,1,0:T(1,128)S(1)} all-gather(f32[1,1,256]{2,1,0:T(1,128)S(1)} %convolution_bitcast_fusion.3), channel_id=3, replica_groups=mesh['sp'=8,'tp'=4] {'sp'}, dimensions={0}, use_global_device_ids=true | all-gather | bytes 9216 | tf_op jit(solution)/shard_map/all_gather | solution.py:16
  207.6 1.9 copy.46
  209.5 3.5 all-to-all-start
  213.4 6.9 %all-to-all-done = bf16[4,192,256]{2,1,0:T(8,128)(2,1)S(1)} async-done(((bf16[4,192,256]{2,1,0:T(8,128)(2,1)}), bf16[4,192,256]{2,1,0:T(8,128)(2,1)S(1)}, u32[]{:S(2)}, u32[]{:S(2)}) %all-to-all-start) | async-done | bytes 393248 | tf_op jit(solution)/shard_map/all_to_all | solution.py:189
  221.5 3.5 multiply_reduce_fusion
  227.1 103.0 %all_to_all.20 = bf16[8,96,2048]{2,1,0:T(8,128)(2,1)S(1)} all-to-all(bf16[8,96,2048]{2,1,0:T(8,128)(2,1)S(1)} %pad_maximum_fusion), channel_id=1, replica_groups=mesh['sp'=8,'tp'=4] {'sp'}, dimensions={0} | all-to-all | bytes 6291456 | tf_op jit(solution)/shard_map/all_to_all | solution.py:231
  330.1 1.7 copy-done.3
  331.8 3.0 fusion.60
  334.9 8.2 %convolution_convert_fusion = bf16[8,96,2048]{2,1,0:T(8,128)(2,1)} fusion(bf16[1,512,2048]{2,1,0:T(8,128)(2,1)S(1)} %copy-done, bf16[8,96,2048]{2,1,0:T(8,128)(2,1)} %copy-done.3, bf16[1,2048,512]{2,1,0:T(8,128)(2,1)} %param.32, f32[8,96,512]{2,1,0:T(8,128)} %fusion.60), kind=kOutput, calls=%fused_computation.78 | convolution fusion | flops 3225157632 | bytes 12058624 | tf_op jit(solution)/shard_map/pesf,efd->pesd/dot_general | solution.py:131
  343.0 4.5 %all-to-all-start.2 = ((bf16[8,96,2048]{2,1,0:T(8,128)(2,1)}), bf16[8,96,2048]{2,1,0:T(8,128)(2,1)}, u32[]{:S(2)}, u32[]{:S(2)}) async-start(bf16[8,96,2048]{2,1,0:T(8,128)(2,1)} %convolution_convert_fusion), calls=%async_computation.2 | async-start | bytes 6291456 | tf_op jit(solution)/shard_map/all_to_all | solution.py:237
  348.1 69.2 %all-to-all-done.2 = bf16[8,96,2048]{2,1,0:T(8,128)(2,1)} async-done(((bf16[8,96,2048]{2,1,0:T(8,128)(2,1)}), bf16[8,96,2048]{2,1,0:T(8,128)(2,1)}, u32[]{:S(2)}, u32[]{:S(2)}) %all-to-all-start.2) | async-done | bytes 3145760 | tf_op jit(solution)/shard_map/all_to_all | solution.py:237
  417.3 2.3 fusion.112
  (290 shorter events, 122.3 us)
Async XLA Ops:
  6.5 328.3 %copy-start = (bf16[1,512,2048]{2,1,0:T(8,128)(2,1)S(1)}, bf16[1,512,2048]{2,1,0:T(8,128)(2,1)}, u32[]{:S(2)}) copy-start(bf16[1,512,2048]{2,1,0:T(8,128)(2,1)} %param.33) | copy-start | bytes 6291460
  6.5 197.2 %all-gather.5.cloned.1.call-start = ((), (), s32[]{:S(2)}) async-start(), calls=%async_computation.3 | async-start | bytes 2359296 | tf_op jit(solution)/shard_map/all_gather | solution.py:16
  8.1 10.4 %copy-start.21 = (f32[6]{0:T(128)}, f32[6]{0:T(128)S(1)}, u32[]{:S(2)}) copy-start(f32[6]{0:T(128)S(1)} %slice_bitcast_fusion) | copy-start | bytes 76
  155.2 26.6 %copy-start.20 = (s32[192,2]{0,1:T(2,128)S(1)}, s32[192,2]{0,1:T(2,128)}, u32[]{:S(2)}) copy-start(s32[192,2]{0,1:T(2,128)} %param.29) | copy-start | bytes 4612
  155.2 30.5 %copy-start.4 = (bf16[12,1,64,256]{3,2,1,0:T(8,128)(2,1)S(1)}, bf16[12,1,64,256]{3,2,1,0:T(8,128)(2,1)}, u32[]{:S(2)}) copy-start(bf16[12,1,64,256]{3,2,1,0:T(8,128)(2,1)} %get-tuple-element.533) | copy-start | bytes 1179652
  182.1 1.1 copy-start.10
  183.1 0.6 copy-start.14
  183.8 19.9 %copy-start.6 = (s32[96,2]{1,0:T(8,128)}, s32[96,2]{1,0:T(8,128)S(1)}, u32[]{:S(2)}) copy-start(s32[96,2]{1,0:T(8,128)S(1)} %copy.55) | copy-start | bytes 2308
  183.9 19.8 %copy-start.12 = (s32[192]{0:T(256)}, s32[192]{0:T(256)S(1)}, u32[]{:S(2)}) copy-start(s32[192]{0:T(256)S(1)} %eq.114) | copy-start | bytes 2308
  184.9 18.8 %copy-start.16 = (s32[192]{0:T(256)}, s32[192]{0:T(256)S(1)}, u32[]{:S(2)}) copy-start(s32[192]{0:T(256)S(1)} %fusion.98) | copy-start | bytes 2308
  203.8 1.0 copy-start.5
  207.6 5.4 %copy-start.7 = (s32[96,2]{1,0:T(8,128)S(1)}, s32[96,2]{1,0:T(8,128)}, u32[]{:S(2)}) copy-start(s32[96,2]{1,0:T(8,128)} %copy-done.6) | copy-start | bytes 2308
  207.6 5.4 %copy-start.8 = (s32[96,2]{1,0:T(8,128)S(1)}, s32[96,2]{1,0:T(8,128)}, u32[]{:S(2)}) copy-start(s32[96,2]{1,0:T(8,128)} %reduce_sum.106) | copy-start | bytes 2308
  207.6 5.4 %copy-start.9 = (s32[96,2]{1,0:T(8,128)S(1)}, s32[96,2]{1,0:T(8,128)}, u32[]{:S(2)}) copy-start(s32[96,2]{1,0:T(8,128)} %multiply_add_fusion.1) | copy-start | bytes 2308
  209.5 10.8 %all-to-all-start = ((bf16[4,192,256]{2,1,0:T(8,128)(2,1)}), bf16[4,192,256]{2,1,0:T(8,128)(2,1)S(1)}, u32[]{:S(2)}, u32[]{:S(2)}) async-start(bf16[4,192,256]{2,1,0:T(8,128)(2,1)} %bitcast.29), calls=%async_computation | async-start | bytes 786432 | tf_op jit(solution)/shard_map/all_to_all | solution.py:189
  213.4 7.3 %copy-start.24 = (bf16[192,1024]{1,0:T(8,128)(2,1)S(1)}, bf16[192,1024]{1,0:T(8,128)(2,1)}, u32[]{:S(2)}) copy-start(bf16[192,1024]{1,0:T(8,128)(2,1)} %param.23) | copy-start | bytes 1179652
  213.4 7.3 %copy-start.25 = (f32[1024]{0:T(1024)S(1)}, f32[1024]{0:T(1024)}, u32[]{:S(2)}) copy-start(f32[1024]{0:T(1024)} %param.26) | copy-start | bytes 12292
  220.3 1.1 copy-start.23
  221.5 3.5 copy-start.18
  224.9 1.2 copy-start.1
  227.1 104.7 %copy-start.22 = (bf16[1,2048,512]{2,1,0:T(8,128)(2,1)S(1)}, bf16[1,2048,512]{2,1,0:T(8,128)(2,1)}, u32[]{:S(2)}) copy-start(bf16[1,2048,512]{2,1,0:T(8,128)(2,1)} %param.31) | copy-start | bytes 6291460
  330.1 1.7 copy-start.3
  343.0 4.5 %copy-start.11 = (s32[192]{0:T(256)S(1)}, s32[192]{0:T(256)}, u32[]{:S(2)}) copy-start(s32[192]{0:T(256)} %copy-done.10) | copy-start | bytes 2308
  343.0 4.5 %copy-start.15 = (s32[192]{0:T(256)S(1)}, s32[192]{0:T(256)}, u32[]{:S(2)}) copy-start(s32[192]{0:T(256)} %copy-done.14) | copy-start | bytes 2308
  343.0 4.7 %copy-start.13 = (s32[192]{0:T(256)S(1)}, s32[192]{0:T(256)}, u32[]{:S(2)}) copy-start(s32[192]{0:T(256)} %copy-done.12) | copy-start | bytes 2308
  343.0 4.7 %copy-start.17 = (s32[192]{0:T(256)S(1)}, s32[192]{0:T(256)}, u32[]{:S(2)}) copy-start(s32[192]{0:T(256)} %copy-done.16) | copy-start | bytes 2308
  343.0 5.0 %copy-start.19 = (f32[192,2]{0,1:T(2,128)S(1)}, f32[192,2]{0,1:T(2,128)}, u32[]{:S(2)}) copy-start(f32[192,2]{0,1:T(2,128)} %param.30) | copy-start | bytes 4612
  343.0 74.3 %all-to-all-start.2 = ((bf16[8,96,2048]{2,1,0:T(8,128)(2,1)}), bf16[8,96,2048]{2,1,0:T(8,128)(2,1)}, u32[]{:S(2)}, u32[]{:S(2)}) async-start(bf16[8,96,2048]{2,1,0:T(8,128)(2,1)} %convolution_convert_fusion), calls=%async_computation.2 | async-start | bytes 6291456 | tf_op jit(solution)/shard_map/all_to_all | solution.py:237
  420.2 1.4 copy-start.2
Sparse Core Ops, SparseCore 0:
  14.3 51.8 all-gather.4
where the time goes:
time: 436 us; the launch traced here: 430 us
  blocking collectives  143 us (33%)
  matrix products  110 us (25%)
  waiting for transfers between devices  76.2 us (17%)
  other arithmetic  35.8 us (8%)
  local copies, waits for them, and re-layouts  27.3 us (6%)
  loops' own time  15.6 us (4%)
  between operations  14 us (3%)
  starting transfers between devices  7.91 us (2%)
    all_to_all x1, blocking collectives, shards(): lax.all_to_all(send_rows, 'sp', split_axis=0, concat_axis=0, tiled=True)  103 us
    all_to_all x1, waiting for transfers between devices, shards(): lax.all_to_all(finished, 'sp', split_axis=0, concat_axis=0, tiled=True)  69.2 us
    unnamed x1, blocking collectives  23.8 us
    dot_general x12, matrix products, block_step(): jnp.dot(keep_weight, k_float, precision=HIGHEST)  18.9 us
    dot_general x12, matrix products, block_step(): jnp.dot(weights_blk, v_block, preferred_element_type=jnp.float32)  18.9 us
    all_gather x1, blocking collectives, prefix(): gathered = jax.tree.map(lambda a: lax.all_gather(a, axis), part)  16.3 us
    another operation x1, loops' own time, block_pass(): lax.scan(block_step, state, (to_blocks(query), to_blocks(keys), to_blocks...  15.6 us
    dot_general x12, matrix products, block_step(): jnp.dot((k_float * keep_weight[:, None]).T, v_block.astype(jnp.float32),...  15.2 us
  transfers between devices with their start and end apart: 3, of which 2 were waited for; matrix products, arithmetic and copies ran while one was open for 31% of the time, Pallas kernels for 0%

commit v1 on v0

v1 whole, which is shorter than its diff:
```python
import functools

import jax
import jax.numpy as jnp
from jax import lax
from jax.experimental import pallas as pl
from jax.experimental.pallas import tpu as pltpu
from jax.sharding import PartitionSpec as P

BLOCK = 64


EPS = 1e-06
FLOOR_LOG = -1e30
HIGHEST = lax.Precision.HIGHEST


EXTRA = 8
VMEM_LIMIT = 56 * 1024 * 1024


def col_mask(first_row, rows, cols):
    row = lax.broadcasted_iota(jnp.int32, (rows, cols), 0) + first_row
    col = lax.broadcasted_iota(jnp.int32, (rows, cols), 1)
    return row, col


def split_two(a):
    high = a.astype(jnp.bfloat16)
    return high, (a - high.astype(jnp.float32)).astype(jnp.bfloat16)


def log_rows(forget_ref, input_ref):
    pre = forget_ref[...]
    log_forget = jnp.minimum(pre, 0.0) - jnp.log1p(jnp.exp(-jnp.abs(pre)))
    seq_len = pre.shape[1]
    row, col = col_mask(0, seq_len, seq_len)
    upper = jnp.where(row <= col, 1.0, 0.0).astype(jnp.bfloat16)
    one, rest = split_two(log_forget)
    two, three = split_two(log_forget - one.astype(jnp.float32))
    stacked = jnp.concatenate([one, two, three, jnp.zeros((13, seq_len), jnp.bfloat16)], axis=0)
    sums = jnp.dot(stacked, upper, preferred_element_type=jnp.float32)
    cum_row = sums[0:1] + sums[1:2] + sums[2:3]
    return log_forget, cum_row, input_ref[...] - cum_row


def cell_state_kernel(k_ref, v_ref, forget_ref, input_ref, state_ref):
    width = k_ref.shape[1]
    seq_len = k_ref.shape[0]
    log_forget, cum_row, gap_row = log_rows(forget_ref, input_ref)
    total = jnp.sum(log_forget, axis=1, keepdims=True)
    top = jnp.max(gap_row, axis=1, keepdims=True)
    keep_row = jnp.exp(gap_row - top) * width ** (-0.5)
    k_turned = k_ref[...].astype(jnp.float32).T
    weighted = k_turned * keep_row
    high, low = split_two(weighted)
    v = v_ref[...]
    state_ref[0:width, :] = jnp.dot(high, v, preferred_element_type=jnp.float32) + jnp.dot(
        low, v, preferred_element_type=jnp.float32
    )
    vector = jnp.dot(
        jnp.broadcast_to(keep_row, (8, seq_len)),
        k_ref[...].astype(jnp.float32),
        precision=HIGHEST,
        preferred_element_type=jnp.float32,
    )[0:1]
    lanes = jnp.zeros((1, width), jnp.float32)
    state_ref[width : width + EXTRA, :] = jnp.concatenate(
        [vector, lanes + total, lanes + total + top, jnp.zeros((EXTRA - 3, width), jnp.float32)],
        axis=0,
    )


def cell_local_kernel(q_ref, k_ref, v_ref, forget_ref, input_ref, num_ref, aux_ref, *, tile):
    seq_len, width = q_ref.shape
    log_forget, cum_row, gap_row = log_rows(forget_ref, input_ref)
    for first in range(0, seq_len, tile):
        span = first + tile
        row, col = col_mask(first, tile, span)
        causal = col <= row
        own = (col // BLOCK) == (row // BLOCK)
        gap = jnp.where(causal, gap_row[:, :span], -jnp.inf)
        top = jnp.max(gap, axis=1, keepdims=True)
        cum = jnp.sum(jnp.where(causal, log_forget[:, :span], 0.0), axis=1, keepdims=True)
        scores = lax.dot_general(
            q_ref[first:span, :],
            k_ref[0:span, :],
            (((1,), (1,)), ((), ())),
            preferred_element_type=jnp.float32,
        ) * width ** (-0.5)
        weights = scores * jnp.exp(gap - top)
        high = weights.astype(jnp.bfloat16)
        high_float = high.astype(jnp.float32)
        low_float = jnp.where(own, 0.0, weights - high_float)
        v = v_ref[0:span, :]
        num_ref[first:span, :] = jnp.dot(high, v, preferred_element_type=jnp.float32) + jnp.dot(
            low_float.astype(jnp.bfloat16), v, preferred_element_type=jnp.float32
        )
        den = jnp.sum(high_float + low_float, axis=1, keepdims=True)
        lane = lax.broadcasted_iota(jnp.int32, (tile, 128), 1)
        aux_ref[first:span, :] = jnp.where(lane == 0, den, jnp.where(lane == 1, top, cum))


def cell_join_kernel(q_ref, num_ref, aux_ref, states_ref, rows_ref, mat_ref, *, axis):
    width = q_ref.shape[1]
    place = lax.axis_index(axis)
    mat_ref[...] = jnp.zeros_like(mat_ref)

    def join(step, carry):
        vector, old_max = carry
        extra = states_ref[step, width : width + EXTRA, :]
        new_max, total = extra[2:3], extra[1:2]
        joined = jnp.maximum(total + old_max, new_max)
        keep_old = jnp.exp(total + old_max - joined)
        keep_new = jnp.exp(new_max - joined)
        mat_ref[...] = keep_old * mat_ref[...] + keep_new * states_ref[step, 0:width, :]
        return keep_old * vector + keep_new * extra[0:1], joined

    vector, far_max = lax.fori_loop(
        0,
        place,
        join,
        (jnp.zeros((1, width), jnp.float32), jnp.full((1, width), FLOOR_LOG, jnp.float32)),
    )
    aux = aux_ref[...]
    den, top, cum = aux[:, 0:1], aux[:, 1:2], aux[:, 2:3]
    far = far_max[:, 0:1]
    joined = jnp.maximum(top, far)
    keep_own = jnp.exp(top - joined)
    keep_far = jnp.exp(far - joined)
    q_float = q_ref[...].astype(jnp.float32)
    one, rest = split_two(mat_ref[...])
    two, three = split_two(mat_ref[...] - one.astype(jnp.float32))
    q = q_ref[...]
    far_num = (
        jnp.dot(q, one, preferred_element_type=jnp.float32)
        + jnp.dot(q, two, preferred_element_type=jnp.float32)
        + jnp.dot(q, three, preferred_element_type=jnp.float32)
    )
    far_den = jnp.sum(q_float * vector, axis=1, keepdims=True)
    numerator = keep_own * num_ref[...] + keep_far * far_num
    denominator = keep_own * den + keep_far * far_den
    divisor = jnp.maximum(jnp.abs(denominator), jnp.exp(-(cum + joined)))
    rows_ref[...] = (numerator / divisor).astype(rows_ref.dtype)


def run_cell(query, keys, values, forget_pre, input_pre, riders):
    seq_len, width = query.shape
    params = pltpu.CompilerParams(vmem_limit_bytes=VMEM_LIMIT)
    state = pl.pallas_call(
        cell_state_kernel,
        out_shape=jax.ShapeDtypeStruct((width + EXTRA, width), jnp.float32),
        compiler_params=params,
        cost_estimate=pl.CostEstimate(flops=10**9, bytes_accessed=2**20, transcendentals=0),
        name="cell_state",
    )(keys, values, forget_pre, input_pre)
    if riders is not None:
        state = jnp.concatenate([state, riders], axis=0)
    gathered = lax.all_gather(state, "sp")
    tile = 4 * BLOCK if seq_len % (4 * BLOCK) == 0 else BLOCK
    numerator, aux = pl.pallas_call(
        functools.partial(cell_local_kernel, tile=tile),
        out_shape=(
            jax.ShapeDtypeStruct((seq_len, width), jnp.float32),
            jax.ShapeDtypeStruct((seq_len, 128), jnp.float32),
        ),
        compiler_params=params,
        cost_estimate=pl.CostEstimate(flops=5 * 10**9, bytes_accessed=2**21, transcendentals=0),
        name="cell_local",
    )(query, keys, values, forget_pre, input_pre)
    rows = pl.pallas_call(
        functools.partial(cell_join_kernel, axis="sp"),
        out_shape=jax.ShapeDtypeStruct((seq_len, width), jnp.bfloat16),
        scratch_shapes=[pltpu.VMEM((width, width), jnp.float32)],
        compiler_params=params,
        name="cell_join",
    )(query, numerator, aux, gathered[:, : width + EXTRA])
    return rows, gathered[:, width + EXTRA :]


def slot_select(expert_ids, expert_count, capacity):
    flat_ids = expert_ids.reshape(-1)
    one_hot = (flat_ids[:, None] == jnp.arange(expert_count, dtype=jnp.int32)[None, :]).astype(
        jnp.int32
    )
    slot_rank = jnp.sum((jnp.cumsum(one_hot, axis=0) - 1) * one_hot, axis=1)
    target = flat_ids * capacity + slot_rank
    return (
        jnp.arange(expert_count * capacity, dtype=jnp.int32)[:, None] == target[None, :]
    ).astype(jnp.bfloat16)


def run_experts(arrived, w_gate, w_up, w_down, sources):
    local_count = w_gate.shape[0]
    grouped = arrived.reshape(sources, local_count, arrived.shape[1], arrived.shape[2])
    gate_pre = jnp.einsum("pesd,edf->pesf", grouped, w_gate, preferred_element_type=jnp.float32)
    up_pre = jnp.einsum("pesd,edf->pesf", grouped, w_up, preferred_element_type=jnp.float32)
    active = (jax.nn.silu(gate_pre) * up_pre).astype(jnp.bfloat16)
    result = jnp.einsum(
        "pesf,efd->pesd", active, w_down, preferred_element_type=jnp.float32
    ).astype(jnp.bfloat16)
    return result.reshape(arrived.shape)


def shards(
    resid,
    query,
    keys,
    values,
    out_gate,
    forget_pre,
    input_pre,
    head_gain,
    out_proj,
    ffn_gain,
    routes,
    route_scores,
    w_gate,
    w_up,
    w_down,
):
    head_width = query.shape[1]
    row_count, route_count = routes.shape
    sources = lax.axis_size("sp")
    local_experts = w_gate.shape[0]
    expert_count = local_experts * sources
    half_rows = row_count // 2
    capacity = max(2, 2 * half_rows * route_count // expert_count)
    whole_rows = local_experts == 1 and row_count <= 2 * expert_count * capacity
    whole_rows = whole_rows and sources * row_count <= 8 * row_count and row_count <= head_width
    route_weight = route_scores / jnp.sum(route_scores, axis=1, keepdims=True)
    riders = None
    if whole_rows:
        named = routes[:, :, None] == jnp.arange(expert_count, dtype=routes.dtype)[None, None, :]
        per_expert = jnp.sum(jnp.where(named, route_weight[:, :, None], 0.0), axis=1).T
        riders = jnp.pad(
            per_expert, ((0, -expert_count % 8), (0, head_width - row_count))
        )
    cell_rows, ridden = run_cell(query, keys, values, forget_pre, input_pre, riders)
    token_rows = lax.all_to_all(cell_rows, "tp", split_axis=0, concat_axis=1, tiled=True)
    cell_float = token_rows.astype(jnp.float32)
    headed = (
        cell_float
        * lax.rsqrt(jnp.mean(cell_float * cell_float, axis=1, keepdims=True) + EPS)
        * head_gain[None, :]
    )
    gated_out = (headed * jax.nn.sigmoid(out_gate.astype(jnp.float32))).astype(jnp.bfloat16)
    after_mix = resid.astype(jnp.float32) + jnp.dot(
        gated_out, out_proj, preferred_element_type=jnp.float32
    )
    normed_rows = (
        after_mix
        * lax.rsqrt(jnp.mean(after_mix * after_mix, axis=1, keepdims=True) + EPS)
        * ffn_gain[None, :]
    ).astype(jnp.bfloat16)
    if whole_rows:
        here = lax.axis_index("sp")
        weights = lax.dynamic_index_in_dim(ridden, here, 1, False)[:, :row_count]
        weights = weights.reshape(sources * row_count, 1)
        arrived = lax.all_gather(normed_rows, "sp", axis=0, tiled=True)
        gate_pre = jnp.dot(arrived, w_gate[0], preferred_element_type=jnp.float32)
        up_pre = jnp.dot(arrived, w_up[0], preferred_element_type=jnp.float32)
        active = (jax.nn.silu(gate_pre) * up_pre).astype(jnp.bfloat16)
        result = jnp.dot(active, w_down[0], preferred_element_type=jnp.float32)
        weighted = (result * weights).astype(jnp.bfloat16)
        combined = lax.psum_scatter(weighted, "sp", scatter_dimension=0, tiled=True)
        return (after_mix + combined.astype(jnp.float32)).astype(jnp.bfloat16)
    selects = [
        slot_select(
            routes[half_idx * half_rows : (half_idx + 1) * half_rows], expert_count, capacity
        )
        for half_idx in range(2)
    ]

    def pack_rows(half_idx):
        selection = (
            selects[half_idx].reshape(expert_count * capacity, half_rows, route_count).sum(axis=2)
        )
        packed = jnp.dot(
            selection,
            normed_rows[half_idx * half_rows : (half_idx + 1) * half_rows],
            preferred_element_type=jnp.float32,
        )
        return packed.astype(jnp.bfloat16).reshape(expert_count, capacity, normed_rows.shape[1])

    send_rows = jnp.concatenate([pack_rows(0), pack_rows(1)], axis=1)
    finished = run_experts(
        lax.all_to_all(send_rows, "sp", split_axis=0, concat_axis=0, tiled=True),
        w_gate,
        w_up,
        w_down,
        sources,
    )
    returned = lax.all_to_all(finished, "sp", split_axis=0, concat_axis=0, tiled=True)
    answers = [returned[:, :capacity], returned[:, capacity:]]
    pieces = []
    for half_idx in range(2):
        gathered = lax.dot_general(
            selects[half_idx],
            answers[half_idx].reshape(expert_count * capacity, -1),
            (((0,), (0,)), ((), ())),
            preferred_element_type=jnp.float32,
        )
        weights_half = route_weight[half_idx * half_rows : (half_idx + 1) * half_rows]
        pieces.append(
            jnp.sum(gathered.reshape(half_rows, route_count, -1) * weights_half[:, :, None], axis=1)
        )
    return (after_mix + jnp.concatenate(pieces, axis=0)).astype(jnp.bfloat16)


def solution(mesh):
    placed = (
        P(("sp", "tp"), None),
        P("sp", "tp"),
        P("sp", "tp"),
        P("sp", "tp"),
        P(("sp", "tp"), None),
        P("tp", "sp"),
        P("tp", "sp"),
        P(),
        P(),
        P(),
        P(("sp", "tp"), None),
        P(("sp", "tp"), None),
        P("sp", None, None),
        P("sp", None, None),
        P("sp", None, None),
    )
    return jax.shard_map(
        shards, mesh=mesh, in_specs=placed, out_specs=P(("sp", "tp"), None), check_vma=False
    )
```

time: 436 us -> 332 us (0.76); the launches traced: 430 us -> 332 us
  waiting for transfers between devices: 76.2 us -> 262 us
  blocking collectives: 143 us -> 11 us
  matrix products: 110 us -> 21.5 us
  other arithmetic: 35.8 us -> 7.88 us
  local copies, waits for them, and re-layouts: 27.3 us -> 5.27 us
  loops' own time: 15.6 us -> 0 us
  Pallas kernels: 0 us -> 10.8 us
  starting transfers between devices: 7.91 us -> 0.09 us
    all_gather x1 -> x2, waiting for transfers between devices: 0.01 us -> 145 us  [the longest x1 95.8 us: shards(): arrived = lax.all_gather(normed_rows, 'sp', axis=0, tiled=True)]
    reduce_scatter x0 -> x1, waiting for transfers between devices: none -> 116 us  [shards(): combined = lax.psum_scatter(weighted, 'sp', scatter_dimension=0, tiled=True)]
    all_to_all x1, blocking collectives: 103 us -> 11 us  [shards(): lax.all_to_all(cell_rows, 'tp', split_axis=0, concat_axis=1, tiled=True)]
    dot_general x82 -> x2, matrix products: 106 us -> 20.2 us  [the longest x1 11.7 us: shards(): result = jnp.dot(active, w_down[0], preferred_element_type=jnp.float32)]
    all_to_all x2 -> x0, waiting for transfers between devices: 76.1 us -> none  [the longest x1 69.2 us: shards(): lax.all_to_all(finished, 'sp', split_axis=0, concat_axis=0, tiled=True)]
    unnamed x1 -> x0, blocking collectives: 23.8 us -> none
    reduce_max x25 -> x0, other arithmetic: 17.8 us -> none  [the longest x12 14.6 us: block_step(): new_max = jnp.maximum(block_total + max_log, jnp.max(log_keep))]
    all_gather x1 -> x0, blocking collectives: 16.3 us -> none  [prefix(): gathered = jax.tree.map(lambda a: lax.all_gather(a, axis), part)]
  transfers between devices with their start and end apart: 3 -> 3, of which waited for: 2 -> 3; matrix products, arithmetic and copies ran while one was open for 31% -> 0% of each run, Pallas kernels for 0% -> 1%
where the time goes in v1:
time: 332 us
  waiting for transfers between devices  262 us (79%)
  matrix products  21.5 us (6%)
  between operations  13.2 us (4%)
  blocking collectives  11 us (3%)
  Pallas kernels  10.8 us (3%)
  other arithmetic  7.88 us (2%)
  local copies, waits for them, and re-layouts  5.27 us (2%)
    reduce_scatter x1, waiting for transfers between devices, shards(): combined = lax.psum_scatter(weighted, 'sp', scatter_dimension=0, tiled=True)  116 us
    all_gather x1, waiting for transfers between devices, shards(): arrived = lax.all_gather(normed_rows, 'sp', axis=0, tiled=True)  95.8 us
    all_gather x1, waiting for transfers between devices, run_cell(): gathered = lax.all_gather(state, 'sp')  49.6 us
    dot_general x1, matrix products, shards(): result = jnp.dot(active, w_down[0], preferred_element_type=jnp.float32)  11.7 us
    all_to_all x1, blocking collectives, shards(): lax.all_to_all(cell_rows, 'tp', split_axis=0, concat_axis=1, tiled=True)  11 us
    dot_general x1, matrix products, shards(): gate_pre = jnp.dot(arrived, w_gate[0], preferred_element_type=jnp.float32)  8.5 us
  transfers between devices with their start and end apart: 3, of which 3 were waited for; matrix products, arithmetic and copies ran while one was open for 0% of the time, Pallas kernels for 1%

profile of v1, /device:TPU:0, one launch (start us, length us, event | category | flops | bytes accessed | tf_op | source)
XLA Modules:
  0.0 331.5 jit_solution(3420608052901664460)
XLA Ops:
  6.5 0.0 copy-start
  6.5 0.8 reduce_sum.36
  7.4 0.7 broadcast_divide_fusion
  8.1 0.7 select_reduce_fusion
  8.8 2.9 cell_state.1
  11.7 1.7 select_maximum_fusion
  13.4 0.0 all-gather.6.cloned.1.call-update
  13.4 0.0 all-gather.4.cloned.1.call-start
  13.5 3.6 %cell_local.1 = (f32[768,256]{1,0:T(8,128)}, f32[768,128]{1,0:T(8,128)}) custom-call(bf16[768,256]{1,0:T(8,128)(2,1)} %q_ref.3, bf16[768,256]{1,0:T(8,128)(2,1)} %k_ref.3, bf16[768,256]{1,0:T(8,128)(2,1)} %v_ref.3, f32[1,768]{1,0:T(1,128)} %forget_ref.3, f32[1,768]{1,0:T(1,128)} %input_ref.3), custom_call_target="tpu_custom_call" | custom-call | flops 5000000000 | bytes 2097152 | tf_op jit(solution)/shard_map/cell_local/pallas_call | solution.py:161
  17.0 49.6 %all-gather.6.cloned.1.call-done = f32[2176,256]{1,0:T(8,128)} async-done(((f32[272,256]{1,0:T(8,128)}), f32[2176,256]{1,0:T(8,128)}) %all-gather.6.cloned.1.call-update) | async-done | bytes 2228240 | tf_op jit(solution)/shard_map/all_gather | solution.py:159
  66.7 3.1 slice.12.states_ref
  69.8 4.2 %cell_join.1 = bf16[768,256]{1,0:T(8,128)(2,1)} custom-call(bf16[768,256]{1,0:T(8,128)(2,1)} %q_ref.3, f32[768,256]{1,0:T(8,128)} %get-tuple-element.7.num_ref, f32[768,128]{1,0:T(8,128)} %get-tuple-element.8.aux_ref, f32[8,264,256]{2,1,0:T(8,128)} %slice.12.states_ref), custom_call_target="tpu_custom_call" | custom-call | tf_op jit(solution)/shard_map/cell_join/pallas_call | solution.py:171
  74.0 11.0 %all_to_all.13 = bf16[4,192,256]{2,1,0:T(8,128)(2,1)S(1)} all-to-all(bf16[4,192,256]{2,1,0:T(8,128)(2,1)} %bitcast.27), channel_id=1, replica_groups=mesh['sp'=8,'tp'=4] {'tp'}, dimensions={0} | all-to-all | bytes 786432 | tf_op jit(solution)/shard_map/all_to_all | solution.py:240
  85.0 0.2 fusion.5
  85.2 0.1 convert_bitcast_fusion
  85.2 0.1 copy.21
  85.3 0.0 copy-done.3
  85.3 0.0 copy-done.4
  85.4 0.0 copy-start.2
  85.4 1.3 multiply_reduce_fusion
  86.7 1.1 copy-done.1
  87.8 1.1 multiply_convert_fusion.1
  88.9 0.0 all-gather.4.cloned.1.call-update
  88.9 0.0 reduce-scatter.2.cloned.1.call-start
  89.0 0.8 slice.13
  89.9 0.1 mul.73
  89.9 95.8 %all-gather.4.cloned.1.call-done = bf16[1536,2048]{1,0:T(8,128)(2,1)} async-done(((bf16[192,2048]{1,0:T(8,128)(2,1)}), bf16[1536,2048]{1,0:T(8,128)(2,1)}) %all-gather.4.cloned.1.call-update) | async-done | bytes 6291472 | tf_op jit(solution)/shard_map/all_gather | solution.py:260
  185.7 8.5 %fusion.3 = f32[1536,512]{1,0:T(8,128)} fusion(bf16[1536,2048]{1,0:T(8,128)(2,1)} %all-gather.4.cloned.1.call-done, bf16[1,2048,512]{2,1,0:T(8,128)(2,1)} %param.27), kind=kOutput, calls=%fused_computation.6 | convolution fusion | flops 3221225472 | bytes 11534336 | tf_op jit(solution)/shard_map/dot_general | solution.py:261
  194.2 11.7 %multiply_convert_fusion = bf16[1536,2048]{1,0:T(8,128)(2,1)} fusion(f32[1536]{0:T(1024)S(1)} %mul.73, bf16[1,512,2048]{2,1,0:T(8,128)(2,1)S(1)} %copy-done, bf16[1536,2048]{1,0:T(8,128)(2,1)} %all-gather.4.cloned.1.call-done, f32[1536,512]{1,0:T(8,128)} %fusion.3, bf16[1,2048,512]{2,1,0:T(8,128)(2,1)} %param.28), kind=kOutput, calls=%fused_computation | convolution fusion | flops 6453460992 | bytes 19929088 | tf_op jit(solution)/shard_map/dot_general | solution.py:264
  205.9 0.0 reduce-scatter.2.cloned.1.call-update
  206.0 116.4 %reduce-scatter.2.cloned.1.call-done = bf16[192,2048]{1,0:T(8,128)(2,1)} async-done(((bf16[1536,2048]{1,0:T(8,128)(2,1)}), bf16[192,2048]{1,0:T(8,128)(2,1)}) %reduce-scatter.2.cloned.1.call-update) | async-done | bytes 786448 | tf_op jit(solution)/shard_map/reduce_scatter | solution.py:266
  322.3 2.7 add_convert_fusion
  (14 shorter events, 0.0 us)
Async XLA Ops:
  6.5 187.7 %copy-start = (bf16[1,512,2048]{2,1,0:T(8,128)(2,1)S(1)}, bf16[1,512,2048]{2,1,0:T(8,128)(2,1)}, u32[]{:S(2)}) copy-start(bf16[1,512,2048]{2,1,0:T(8,128)(2,1)} %param.29) | copy-start | bytes 6291460
  6.5 60.1 %all-gather.6.cloned.1.call-start = ((), (), s32[]{:S(2)}) async-start(), calls=%async_computation.4 | async-start | bytes 2506752 | tf_op jit(solution)/shard_map/all_gather | solution.py:159
  13.4 172.3 %all-gather.4.cloned.1.call-start = ((), (), s32[]{:S(2)}) async-start(), calls=%async_computation.2 | async-start | bytes 7077888 | tf_op jit(solution)/shard_map/all_gather | solution.py:260
  69.8 15.5 %copy-start.3 = (bf16[1024,2048]{1,0:T(8,128)(2,1)S(1)}, bf16[1024,2048]{1,0:T(8,128)(2,1)}, u32[]{:S(2)}) copy-start(bf16[1024,2048]{1,0:T(8,128)(2,1)} %param.23) | copy-start | bytes 12582916
  74.0 11.3 %copy-start.4 = (bf16[192,2048]{1,0:T(8,128)(2,1)S(1)}, bf16[192,2048]{1,0:T(8,128)(2,1)}, u32[]{:S(2)}) copy-start(bf16[192,2048]{1,0:T(8,128)(2,1)} %param.15) | copy-start | bytes 2359300
  74.0 11.3 %copy-start.5 = (bf16[192,1024]{1,0:T(8,128)(2,1)S(1)}, bf16[192,1024]{1,0:T(8,128)(2,1)}, u32[]{:S(2)}) copy-start(bf16[192,1024]{1,0:T(8,128)(2,1)} %param.19) | copy-start | bytes 1179652
  74.0 11.3 %copy-start.6 = (f32[1024]{0:T(1024)S(1)}, f32[1024]{0:T(1024)}, u32[]{:S(2)}) copy-start(f32[1024]{0:T(1024)} %param.22) | copy-start | bytes 12292
  85.4 2.5 copy-start.2
  86.7 1.1 copy-start.1
  88.9 233.4 %reduce-scatter.2.cloned.1.call-start = ((), (), s32[]{:S(2)}) async-start(), calls=%async_computation.3 | async-start | bytes 7077888 | tf_op jit(solution)/shard_map/reduce_scatter | solution.py:266
Sparse Core Ops, SparseCore 0:
  13.5 53.1 all-gather.5
  89.1 96.5 all-gather.3
  206.1 116.2 reduce-scatter.1

commit v2 on v1

--- a/solution.py
+++ b/solution.py
@@ -144,7 +144,7 @@
     rows_ref[...] = (numerator / divisor).astype(rows_ref.dtype)
 
 
-def run_cell(query, keys, values, forget_pre, input_pre, riders):
+def run_cell(query, keys, values, forget_pre, input_pre):
     seq_len, width = query.shape
     params = pltpu.CompilerParams(vmem_limit_bytes=VMEM_LIMIT)
     state = pl.pallas_call(
@@ -154,9 +154,9 @@
         cost_estimate=pl.CostEstimate(flops=10**9, bytes_accessed=2**20, transcendentals=0),
         name="cell_state",
     )(keys, values, forget_pre, input_pre)
-    if riders is not None:
-        state = jnp.concatenate([state, riders], axis=0)
-    gathered = lax.all_gather(state, "sp")
+    cut = (width + EXTRA) // 3
+    parts = [lax.all_gather(state[i * cut : (i + 1) * cut], "sp") for i in range(3)]
+    gathered = jnp.concatenate(parts, axis=1)
     tile = 4 * BLOCK if seq_len % (4 * BLOCK) == 0 else BLOCK
     numerator, aux = pl.pallas_call(
         functools.partial(cell_local_kernel, tile=tile),
@@ -174,8 +174,8 @@
         scratch_shapes=[pltpu.VMEM((width, width), jnp.float32)],
         compiler_params=params,
         name="cell_join",
-    )(query, numerator, aux, gathered[:, : width + EXTRA])
-    return rows, gathered[:, width + EXTRA :]
+    )(query, numerator, aux, gathered)
+    return rows
 
 
 def slot_select(expert_ids, expert_count, capacity):
@@ -188,6 +188,54 @@
     return (
         jnp.arange(expert_count * capacity, dtype=jnp.int32)[:, None] == target[None, :]
     ).astype(jnp.bfloat16)
+
+
+def exchange_kernel(send_ref, recv_ref, send_sems, recv_sems, own_sem, *, axis, count):
+    place = lax.axis_index(axis)
+    barrier = pltpu.get_barrier_semaphore()
+    for step in range(1, count):
+        peer = lax.rem(place + step, count)
+        pl.semaphore_signal(
+            barrier, inc=1, device_id={axis: peer}, device_id_type=pl.DeviceIdType.MESH
+        )
+    own = pltpu.make_async_copy(send_ref.at[place], recv_ref.at[place], own_sem)
+    own.start()
+    pl.semaphore_wait(barrier, count - 1)
+    copies = []
+    for step in range(1, count):
+        peer = lax.rem(place + step, count)
+        copy = pltpu.make_async_remote_copy(
+            src_ref=send_ref.at[peer],
+            dst_ref=recv_ref.at[place],
+            send_sem=send_sems.at[step - 1],
+            recv_sem=recv_sems.at[step - 1],
+            device_id={axis: peer},
+            device_id_type=pl.DeviceIdType.MESH,
+        )
+        copy.start()
+        copies.append(copy)
+    own.wait()
+    for copy in copies:
+        copy.wait()
+
+
+def exchange(blocks, axis, collective_id):
+    count = lax.axis_size(axis)
+    grouped = blocks.reshape((count, -1) + blocks.shape[2:])
+    out = pl.pallas_call(
+        functools.partial(exchange_kernel, axis=axis, count=count),
+        out_shape=jax.ShapeDtypeStruct(grouped.shape, grouped.dtype),
+        in_specs=[pl.BlockSpec(memory_space=pl.ANY)],
+        out_specs=pl.BlockSpec(memory_space=pl.ANY),
+        scratch_shapes=[
+            pltpu.SemaphoreType.DMA((count - 1,)),
+            pltpu.SemaphoreType.DMA((count - 1,)),
+            pltpu.SemaphoreType.DMA(()),
+        ],
+        compiler_params=pltpu.CompilerParams(collective_id=collective_id, has_side_effects=True),
+        name="exchange",
+    )(grouped)
+    return out.reshape(blocks.shape)
 
 
 def run_experts(arrived, w_gate, w_up, w_down, sources):
@@ -226,17 +274,8 @@
     expert_count = local_experts * sources
     half_rows = row_count // 2
     capacity = max(2, 2 * half_rows * route_count // expert_count)
-    whole_rows = local_experts == 1 and row_count <= 2 * expert_count * capacity
-    whole_rows = whole_rows and sources * row_count <= 8 * row_count and row_count <= head_width
     route_weight = route_scores / jnp.sum(route_scores, axis=1, keepdims=True)
-    riders = None
-    if whole_rows:
-        named = routes[:, :, None] == jnp.arange(expert_count, dtype=routes.dtype)[None, None, :]
-        per_expert = jnp.sum(jnp.where(named, route_weight[:, :, None], 0.0), axis=1).T
-        riders = jnp.pad(
-            per_expert, ((0, -expert_count % 8), (0, head_width - row_count))
-        )
-    cell_rows, ridden = run_cell(query, keys, values, forget_pre, input_pre, riders)
+    cell_rows = run_cell(query, keys, values, forget_pre, input_pre)
     token_rows = lax.all_to_all(cell_rows, "tp", split_axis=0, concat_axis=1, tiled=True)
     cell_float = token_rows.astype(jnp.float32)
     headed = (
@@ -253,18 +292,6 @@
         * lax.rsqrt(jnp.mean(after_mix * after_mix, axis=1, keepdims=True) + EPS)
         * ffn_gain[None, :]
     ).astype(jnp.bfloat16)
-    if whole_rows:
-        here = lax.axis_index("sp")
-        weights = lax.dynamic_index_in_dim(ridden, here, 1, False)[:, :row_count]
-        weights = weights.reshape(sources * row_count, 1)
-        arrived = lax.all_gather(normed_rows, "sp", axis=0, tiled=True)
-        gate_pre = jnp.dot(arrived, w_gate[0], preferred_element_type=jnp.float32)
-        up_pre = jnp.dot(arrived, w_up[0], preferred_element_type=jnp.float32)
-        active = (jax.nn.silu(gate_pre) * up_pre).astype(jnp.bfloat16)
-        result = jnp.dot(active, w_down[0], preferred_element_type=jnp.float32)
-        weighted = (result * weights).astype(jnp.bfloat16)
-        combined = lax.psum_scatter(weighted, "sp", scatter_dimension=0, tiled=True)
-        return (after_mix + combined.astype(jnp.float32)).astype(jnp.bfloat16)
     selects = [
         slot_select(
             routes[half_idx * half_rows : (half_idx + 1) * half_rows], expert_count, capacity
@@ -285,13 +312,13 @@
 
     send_rows = jnp.concatenate([pack_rows(0), pack_rows(1)], axis=1)
     finished = run_experts(
-        lax.all_to_all(send_rows, "sp", split_axis=0, concat_axis=0, tiled=True),
+        exchange(send_rows, "sp", 1),
         w_gate,
         w_up,
         w_down,
         sources,
     )
-    returned = lax.all_to_all(finished, "sp", split_axis=0, concat_axis=0, tiled=True)
+    returned = exchange(finished, "sp", 2)
     answers = [returned[:, :capacity], returned[:, capacity:]]
     pieces = []
     for half_idx in range(2):

time: 332 us -> 292 us (0.88)
  the two profiles are of different devices: /device:TPU:0 before, /device:TPU:12 now
where the time goes in v2:
time: 292 us
  Pallas kernels  157 us (54%)
  blocking collectives  93.7 us (32%)
  matrix products  19.6 us (7%)
  other arithmetic  7.08 us (2%)
  local copies, waits for them, and re-layouts  6.91 us (2%)
  starting transfers between devices  3.77 us (1%)
  waiting for transfers between devices  3.43 us (1%)
    pallas_call x2, Pallas kernels, exchange(): pl.pallas_call(functools.partial(exchange_kernel, axis=axis, count=count)...  146 us
    all_gather x3, blocking collectives, run_cell(): lax.all_gather(state[i * cut:(i + 1) * cut], 'sp')  93.7 us
    dot_general x1, matrix products, run_experts(): jnp.einsum('pesf,efd->pesd', active, w_down, preferred_element_type=jnp.f...  8.17 us
  transfers between devices with their start and end apart: 1, of which 1 were waited for; matrix products, arithmetic and copies ran while one was open for 1% of the time, Pallas kernels for 0%

profile of v2, /device:TPU:12, one launch (start us, length us, event | category | flops | bytes accessed | tf_op | source)
XLA Modules:
  0.0 291.6 jit_solution(14992066985104962924)
XLA Ops:
  0.0 3.1 %cell_state.1 = f32[264,256]{1,0:T(8,128)} custom-call(bf16[768,256]{1,0:T(8,128)(2,1)} %k_ref.3, bf16[768,256]{1,0:T(8,128)(2,1)} %v_ref.3, f32[1,768]{1,0:T(1,128)} %forget_ref.3, f32[1,768]{1,0:T(1,128)} %input_ref.3), custom_call_target="tpu_custom_call" | custom-call | flops 1000000000 | bytes 1048576 | tf_op jit(solution)/shard_map/cell_state/pallas_call | solution.py:150
  3.1 1.0 fusion.38
  4.1 30.4 %all-gather = f32[704,256]{1,0:T(8,128)S(1)} all-gather(f32[88,256]{1,0:T(8,128)S(1)} %get-tuple-element.11), channel_id=2, replica_groups=mesh['sp'=8,'tp'=4] {'sp'}, dimensions={0}, use_global_device_ids=true | all-gather | bytes 811008 | tf_op jit(solution)/shard_map/all_gather | solution.py:158
  34.5 32.4 %all-gather.1 = f32[704,256]{1,0:T(8,128)S(1)} all-gather(f32[88,256]{1,0:T(8,128)S(1)} %get-tuple-element.13), channel_id=3, replica_groups=mesh['sp'=8,'tp'=4] {'sp'}, dimensions={0}, use_global_device_ids=true | all-gather | bytes 811008 | tf_op jit(solution)/shard_map/all_gather | solution.py:158
  66.8 31.0 %all-gather.2 = f32[704,256]{1,0:T(8,128)S(1)} all-gather(f32[88,256]{1,0:T(8,128)S(1)} %get-tuple-element.12), channel_id=4, replica_groups=mesh['sp'=8,'tp'=4] {'sp'}, dimensions={0}, use_global_device_ids=true | all-gather | bytes 811008 | tf_op jit(solution)/shard_map/all_gather | solution.py:158
  97.8 3.6 %cell_local.1 = (f32[768,256]{1,0:T(8,128)}, f32[768,128]{1,0:T(8,128)}) custom-call(bf16[768,256]{1,0:T(8,128)(2,1)} %q_ref.3, bf16[768,256]{1,0:T(8,128)(2,1)} %k_ref.3, bf16[768,256]{1,0:T(8,128)(2,1)} %v_ref.3, f32[1,768]{1,0:T(1,128)} %forget_ref.3, f32[1,768]{1,0:T(1,128)} %input_ref.3), custom_call_target="tpu_custom_call" | custom-call | flops 5000000000 | bytes 2097152 | tf_op jit(solution)/shard_map/cell_local/pallas_call | solution.py:161
  101.4 1.5 pad_maximum_fusion.1.states_ref
  102.9 4.2 %cell_join.1 = bf16[768,256]{1,0:T(8,128)(2,1)} custom-call(bf16[768,256]{1,0:T(8,128)(2,1)} %q_ref.3, f32[768,256]{1,0:T(8,128)} %get-tuple-element.7.num_ref, f32[768,128]{1,0:T(8,128)} %get-tuple-element.8.aux_ref, f32[8,264,256]{2,1,0:T(8,128)} %pad_maximum_fusion.1.states_ref), custom_call_target="tpu_custom_call" | custom-call | tf_op jit(solution)/shard_map/cell_join/pallas_call | solution.py:171
  107.2 3.8 %all-to-all-start = ((bf16[4,192,256]{2,1,0:T(8,128)(2,1)}), bf16[4,192,256]{2,1,0:T(8,128)(2,1)S(1)}, u32[]{:S(2)}, u32[]{:S(2)}) async-start(bf16[4,192,256]{2,1,0:T(8,128)(2,1)} %bitcast.97), calls=%async_computation | async-start | bytes 786432 | tf_op jit(solution)/shard_map/all_to_all | solution.py:279
  111.3 0.6 reduce-window.14
  111.9 0.2 slice_reduce_fusion.1
  112.3 0.1 reduce_sum.93
  112.7 0.6 reduce-window.16
  113.3 0.2 slice_reduce_fusion
  114.7 3.4 %all-to-all-done = bf16[4,192,256]{2,1,0:T(8,128)(2,1)S(1)} async-done(((bf16[4,192,256]{2,1,0:T(8,128)(2,1)}), bf16[4,192,256]{2,1,0:T(8,128)(2,1)S(1)}, u32[]{:S(2)}, u32[]{:S(2)}) %all-to-all-start) | async-done | bytes 393248 | tf_op jit(solution)/shard_map/all_to_all | solution.py:279
  118.3 0.2 fusion.17
  118.5 0.8 copy-done.6
  119.3 3.5 %multiply_reduce_fusion = (f32[192]{0:T(256)S(1)}, f32[192,2048]{1,0:T(8,128)S(1)}) fusion(bf16[1024,2048]{1,0:T(8,128)(2,1)} %param.23, bf16[192,1024]{1,0:T(8,128)(2,1)S(1)} %copy-done.7, f32[192,1024]{1,0:T(8,128)S(1)} %bitcast.98, f32[1024]{0:T(1024)S(1)} %copy-done.8, f32[192]{0:T(256)S(1)} %add_rsqrt_fusion.1, bf16[192,2048]{1,0:T(8,128)(2,1)S(1)} %copy-done.6), kind=kOutput, calls=%fused_computation.23 | convolution fusion | flops 808451904 | bytes 7738880 | tf_op jit(solution)/shard_map/dot_general | solution.py:287
  122.8 0.2 multiply_convert_fusion
  123.0 0.6 convolution_convert_fusion.2
  123.6 0.3 copy-done.1
  123.9 0.6 convolution_convert_fusion.1
  124.5 2.1 pad_maximum_fusion.send_ref
  126.6 74.4 %exchange.2 = bf16[8,96,2048]{2,1,0:T(8,128)(2,1)} custom-call(bf16[8,96,2048]{2,1,0:T(8,128)(2,1)} %pad_maximum_fusion.send_ref), custom_call_target="tpu_custom_call" | custom-call | tf_op jit(solution)/shard_map/exchange/pallas_call | solution.py:225
  201.0 5.6 %fusion.3 = f32[8,96,512]{2,1,0:T(8,128)} fusion(bf16[8,96,2048]{2,1,0:T(8,128)(2,1)} %exchange.2, bf16[1,2048,512]{2,1,0:T(8,128)(2,1)} %param.27), kind=kOutput, calls=%fused_computation.11 | convolution fusion | flops 1610612736 | bytes 6815744 | tf_op jit(solution)/shard_map/pesd,edf->pesf/dot_general | solution.py:244
  206.6 8.2 %convolution_convert_fusion.send_ref = bf16[8,96,2048]{2,1,0:T(8,128)(2,1)} fusion(bf16[1,512,2048]{2,1,0:T(8,128)(2,1)S(1)} %copy-done, bf16[8,96,2048]{2,1,0:T(8,128)(2,1)} %exchange.2, bf16[1,2048,512]{2,1,0:T(8,128)(2,1)} %param.28, f32[8,96,512]{2,1,0:T(8,128)} %fusion.3), kind=kOutput, calls=%fused_computation | convolution fusion | flops 3225157632 | bytes 12058624 | tf_op jit(solution)/shard_map/pesf,efd->pesd/dot_general | solution.py:247
  214.8 71.4 %exchange.3 = bf16[8,96,2048]{2,1,0:T(8,128)(2,1)} custom-call(bf16[8,96,2048]{2,1,0:T(8,128)(2,1)} %convolution_convert_fusion.send_ref), custom_call_target="tpu_custom_call" | custom-call | tf_op jit(solution)/shard_map/exchange/pallas_call | solution.py:225
  286.2 2.3 fusion.37
  288.5 0.6 fusion.12
  289.1 0.6 fusion.13
  289.7 0.8 copy-done.2
  290.5 1.1 fusion.5
  (52 shorter events, 2.1 us)
Async XLA Ops:
  0.0 206.6 %copy-start = (bf16[1,512,2048]{2,1,0:T(8,128)(2,1)S(1)}, bf16[1,512,2048]{2,1,0:T(8,128)(2,1)}, u32[]{:S(2)}) copy-start(bf16[1,512,2048]{2,1,0:T(8,128)(2,1)} %param.29) | copy-start | bytes 6291460
  102.9 8.0 %copy-start.5 = (s32[192,2]{0,1:T(2,128)S(1)}, s32[192,2]{0,1:T(2,128)}, u32[]{:S(2)}) copy-start(s32[192,2]{0,1:T(2,128)} %param.25) | copy-start | bytes 4612
  107.2 7.1 %copy-start.4 = (f32[192,2]{0,1:T(2,128)S(1)}, f32[192,2]{0,1:T(2,128)}, u32[]{:S(2)}) copy-start(f32[192,2]{0,1:T(2,128)} %param.26) | copy-start | bytes 4612
  107.2 11.0 %all-to-all-start = ((bf16[4,192,256]{2,1,0:T(8,128)(2,1)}), bf16[4,192,256]{2,1,0:T(8,128)(2,1)S(1)}, u32[]{:S(2)}, u32[]{:S(2)}) async-start(bf16[4,192,256]{2,1,0:T(8,128)(2,1)} %bitcast.97), calls=%async_computation | async-start | bytes 786432 | tf_op jit(solution)/shard_map/all_to_all | solution.py:279
  114.7 3.8 %copy-start.7 = (bf16[192,1024]{1,0:T(8,128)(2,1)S(1)}, bf16[192,1024]{1,0:T(8,128)(2,1)}, u32[]{:S(2)}) copy-start(bf16[192,1024]{1,0:T(8,128)(2,1)} %param.19) | copy-start | bytes 1179652
  114.7 3.8 %copy-start.8 = (f32[1024]{0:T(1024)S(1)}, f32[1024]{0:T(1024)}, u32[]{:S(2)}) copy-start(f32[1024]{0:T(1024)} %param.22) | copy-start | bytes 12292
  118.2 1.1 copy-start.6
  119.3 3.5 %copy-start.3 = (f32[2048]{0:T(1024)S(1)}, f32[2048]{0:T(1024)}, u32[]{:S(2)}) copy-start(f32[2048]{0:T(1024)} %param.24) | copy-start | bytes 24580
  122.8 1.2 copy-start.1
  289.1 1.4 copy-start.2
